TPU v7x, 32 devices: a whole 2x2x4 slice. The times are simulated.
32 devices in a mesh: sp: 16 (over z, y, x), tp: 2 (over core).
Axes of the slice: x: 2, y: 2, z: 4, core: 2. Of those that a mesh axis runs over, the one named last changes fastest.
Arguments:
- tokens: bfloat16 [2048, 2048], P('sp'), may hold values from -6 to 6
- norm_gain: float32 [2048], replicated, may hold values from 0.1 to 1.9
- conv_value_weight: bfloat16 [2048, 1024], P('sp', 'tp'), may hold values from -0.125 to 0.125
- conv_gate_weight: bfloat16 [2048, 1024], P('sp', 'tp'), may hold values from -0.125 to 0.125
- conv_kernel: float32 [31, 1024], P(None, 'tp'), may hold values from -10 to 10
- conv_bias: float32 [1024], P('tp'), may hold values from -4 to 4
- channel_gain: float32 [1024], P('tp'), may hold values from 0.1 to 1.9
- query_weight: bfloat16 [2048, 2048], P('sp', 'tp'), may hold values from -0.125 to 0.125
- key_weight: bfloat16 [2048, 2048], P('sp', 'tp'), may hold values from -0.125 to 0.125
- value_weight: bfloat16 [2048, 4096], P('sp', 'tp'), may hold values from -0.125 to 0.125
- gate_weight: bfloat16 [2048, 32], replicated, may hold values from -0.125 to 0.125
- gate_offset: float32 [2, 2, 8, 2048], P(None, None, 'tp', 'sp'), may hold values from -110 to 160, as said below
- start_memory: float32 [2, 8, 512, 256], P(None, 'tp'), may hold values from -0.375 to 0.375
- start_norm: float32 [2, 8, 256], P(None, 'tp'), may hold values from -0.375 to 0.375
- start_level: float32 [2, 8], P(None, 'tp'), may hold values from 2 to 5
- cell_gain: float32 [4096], P('tp'), may hold values from 0.1 to 1.9
- out_conv_weight: bfloat16 [2048, 1024], P('sp', 'tp'), may hold values from -0.25 to 0.25
- out_cell_weight: bfloat16 [2048, 4096], P('sp', 'tp'), may hold values from -0.09375 to 0.09375
Outputs:
- mixed: bfloat16 [2048, 2048], P(('sp', 'tp'))
Inputs may be any that keep to these rules, and one draw needn't show every extreme that they name: `gate_offset`: added to the gate pre-activations; index 0 of the second dimension is the input gate, index 1 the forget gate.
All inputs are finite; a program needn't handle non-finite values.
Results may differ from a plain program's by a relative error of at most 0.017.
Values may be sent and summed in bfloat16 or wider, within the bound.
A program may use at most 192 MiB of HBM per device.

v0:
```python
import jax
import jax.numpy as jnp
from jax import lax
from jax.sharding import PartitionSpec as P

CONV_W = 1024
BLOCK = 128


EPS = 1e-06
FLOOR_LEVEL = -1e30
HIGHEST = lax.Precision.HIGHEST


def with_halo(value, sides, width):
    for axis, dim in sides:
        count, length = (lax.axis_size(axis), value.shape[dim])
        up = [(i, (i + 1) % count) for i in range(count - 1)]
        down = [(j, i) for i, j in up]
        last = lax.slice_in_dim(value, length - width, length, axis=dim)
        initial = lax.slice_in_dim(value, 0, width, axis=dim)
        before = lax.ppermute(last, axis, up)
        after = lax.ppermute(initial, axis, down)
        value = jnp.concatenate([before, value, after], axis=dim)
    return value


def entering(part, axis, combine, identity, reverse):
    count = lax.axis_size(axis)
    place = lax.axis_index(axis)
    ahead = count - 1 - place if reverse else place
    gathered = jax.tree.map(lambda a: lax.all_gather(a, axis), part)
    state = jax.tree.map(lambda a, e: jnp.zeros_like(a) + jnp.asarray(e, a.dtype), part, identity)

    def one(turn, state):
        source = count - 1 - turn if reverse else turn
        return combine(
            state, jax.tree.map(lambda a: lax.dynamic_index_in_dim(a, source, 0, False), gathered)
        )

    return lax.fori_loop(0, ahead, one, state)


def back_to_wide(values):
    return lax.optimization_barrier(values.astype(jnp.bfloat16)).astype(jnp.float32)


def block_step(carried, inputs):
    memory, normer, run_level, passed = carried
    queries, key_rows, value_rows, in_gate, log_forget = inputs
    length = queries.shape[1]
    lower_mask = jnp.arange(length)[:, None] >= jnp.arange(length)[None, :]
    cumulative = jnp.cumsum(log_forget, axis=1)
    decay_table = jnp.where(
        lower_mask, cumulative[:, :, None] - cumulative[:, None, :] + in_gate[:, None, :], -jnp.inf
    )
    carried_level = cumulative + run_level[:, None]
    top_level = jnp.maximum(carried_level, jnp.max(decay_table, axis=2))
    carry_weight = jnp.exp(carried_level - top_level)
    scores = jnp.einsum("hbd,hsd->hbs", queries, key_rows, precision=HIGHEST) * jnp.exp(
        decay_table - top_level[:, :, None]
    )
    numerator = jnp.einsum("hbs,hsv->hbv", scores, value_rows, precision=HIGHEST) + carry_weight[
        :, :, None
    ] * jnp.einsum("hvd,hbd->hbv", memory, queries, precision=HIGHEST)
    denominator = jnp.sum(scores, axis=2) + carry_weight * jnp.einsum(
        "hd,hbd->hb", normer, queries, precision=HIGHEST
    )
    block_total = cumulative[:, -1]
    tail_level = block_total[:, None] - cumulative + in_gate
    new_level = jnp.maximum(block_total + run_level, jnp.max(tail_level, axis=1))
    old_weight = jnp.exp(block_total + run_level - new_level)
    new_weight = jnp.exp(tail_level - new_level[:, None])
    memory = old_weight[:, None, None] * memory + jnp.einsum(
        "hbv,hbd->hvd", value_rows * new_weight[:, :, None], key_rows, precision=HIGHEST
    )
    normer = old_weight[:, None] * normer + jnp.einsum(
        "hb,hbd->hd", new_weight, key_rows, precision=HIGHEST
    )
    return (
        (memory, normer, new_level, passed + block_total),
        (numerator, denominator, top_level, cumulative + passed[:, None]),
    )


def local_pass(queries, key_rows, value_rows, in_gate, log_forget):
    heads_here, length, key_width = queries.shape
    value_width = value_rows.shape[2]
    blocks = length // BLOCK

    def to_blocks(values):
        return jnp.moveaxis(values.reshape((heads_here, blocks, BLOCK) + values.shape[2:]), 1, 0)

    def from_blocks(values):
        return jnp.moveaxis(values, 0, 1).reshape((heads_here, length) + values.shape[3:])

    first_state = (
        jnp.zeros((heads_here, value_width, key_width), jnp.float32),
        jnp.zeros((heads_here, key_width), jnp.float32),
        jnp.full((heads_here,), FLOOR_LEVEL, jnp.float32),
        jnp.zeros((heads_here,), jnp.float32),
    )
    summary, outputs = lax.scan(
        block_step,
        first_state,
        tuple(
            (to_blocks(values) for values in (queries, key_rows, value_rows, in_gate, log_forget))
        ),
    )
    return (summary, tuple((from_blocks(values) for values in outputs)))


def join_states(earlier, later):
    memory_first, normer_first, level_first, passed_first = earlier
    memory_second, normer_second, level_second, passed_second = later
    shifted = level_first + passed_second
    joined_level = jnp.maximum(shifted, level_second)
    weight_first = jnp.exp(shifted - joined_level)
    weight_second = jnp.exp(level_second - joined_level)
    joined_memory = (
        weight_first[:, None, None] * memory_first + weight_second[:, None, None] * memory_second
    )
    joined_normer = weight_first[:, None] * normer_first + weight_second[:, None] * normer_second
    return (joined_memory, joined_normer, joined_level, passed_first + passed_second)


def finish(local_out, carried, queries):
    numerator, denominator, top_level, forget_sum = local_out
    memory, normer, run_level, unused = carried
    entry_level = forget_sum + run_level[:, None]
    high_level = jnp.maximum(top_level, entry_level)
    own_weight = jnp.exp(top_level - high_level)
    entry_weight = jnp.exp(entry_level - high_level)
    numerator = own_weight[:, :, None] * numerator + entry_weight[:, :, None] * jnp.einsum(
        "hvd,htd->htv", memory, queries, precision=HIGHEST
    )
    denominator = own_weight * denominator + entry_weight * jnp.einsum(
        "hd,htd->ht", normer, queries, precision=HIGHEST
    )
    return numerator / jnp.maximum(jnp.abs(denominator), 1.0)[:, :, None]


def shards(
    tokens,
    norm_gain,
    conv_value_weight,
    conv_gate_weight,
    conv_kernel,
    conv_bias,
    channel_gain,
    query_weight,
    key_weight,
    value_weight,
    gate_weight,
    gate_offset,
    start_memory,
    start_norm,
    start_level,
    cell_gain,
    out_conv_weight,
    out_cell_weight,
):
    rows_here = tokens.shape[0]
    features = tokens.astype(jnp.float32)
    normed = (
        features * lax.rsqrt(jnp.mean(features * features, axis=1, keepdims=True) + EPS) * norm_gain
    ).astype(jnp.bfloat16)
    pieces = (
        lax.all_gather(conv_value_weight, "sp", axis=0, tiled=True),
        lax.all_gather(conv_gate_weight, "sp", axis=0, tiled=True),
        lax.all_gather(query_weight, "sp", axis=0, tiled=True),
        lax.all_gather(key_weight, "sp", axis=0, tiled=True),
        lax.all_gather(value_weight, "sp", axis=0, tiled=True),
    )
    projected = tuple(
        (
            jnp.dot(normed, weight_piece, preferred_element_type=jnp.float32)
            for weight_piece in pieces
        )
    )
    conv_out_weight, cell_out_weight = (
        lax.all_gather(out_conv_weight, "sp", axis=0, tiled=True),
        lax.all_gather(out_cell_weight, "sp", axis=0, tiled=True),
    )
    conv_value = projected[0].astype(jnp.bfloat16)
    conv_gate = projected[1].astype(jnp.bfloat16)
    gated_rows = (
        conv_value.astype(jnp.float32) * jax.nn.sigmoid(conv_gate.astype(jnp.float32))
    ).astype(jnp.bfloat16)
    half_reach = conv_kernel.shape[0] // 2
    padded = with_halo(gated_rows, (("sp", 0),), half_reach).astype(jnp.float32)
    conv_sum = conv_bias + sum(
        (
            conv_kernel[offset] * padded[offset : offset + rows_here]
            for offset in range(conv_kernel.shape[0])
        )
    )
    channel_total, channel_squares = lax.psum(
        (jnp.sum(conv_sum, axis=1), jnp.sum(conv_sum * conv_sum, axis=1)), "tp"
    )
    channel_mean = channel_total / CONV_W
    channel_var = channel_squares / CONV_W - channel_mean * channel_mean
    conv_out = jax.nn.silu(
        (conv_sum - channel_mean[:, None]) * lax.rsqrt(channel_var + EPS)[:, None] * channel_gain
    ).astype(jnp.bfloat16)
    heads_here = start_level.shape[1]
    key_width = start_norm.shape[2]
    value_width = start_memory.shape[2]

    def split_heads(flat_rows, head_width):
        return jnp.transpose(
            back_to_wide(flat_rows).reshape(rows_here, heads_here, head_width), (1, 0, 2)
        )

    queries = split_heads(projected[2], key_width)
    key_rows = split_heads(projected[3], key_width) * key_width ** (-0.5)
    value_rows = split_heads(projected[4], value_width)
    gate_pre = jnp.dot(normed, gate_weight, preferred_element_type=jnp.float32)
    gate_pre = gate_pre.reshape(rows_here, 2, 2, gate_weight.shape[1] // 4)
    gate_pre = lax.dynamic_slice_in_dim(gate_pre, lax.axis_index("tp") * heads_here, heads_here, 3)
    gate_pre = jnp.transpose(gate_pre, (1, 2, 3, 0)) + gate_offset
    in_gate = gate_pre[:, 0]
    log_forget = jax.nn.log_sigmoid(gate_pre[:, 1])
    forward_summary, forward_local = local_pass(
        queries, key_rows, value_rows, in_gate[0], log_forget[0]
    )
    flipped_queries = jnp.flip(queries, axis=1)
    backward_summary, backward_local = local_pass(
        flipped_queries,
        jnp.flip(key_rows, axis=1),
        jnp.flip(value_rows, axis=1),
        jnp.flip(in_gate[1], axis=1),
        jnp.flip(log_forget[1], axis=1),
    )
    forward_memory, forward_normer, forward_level, forward_passed = forward_summary
    backward_memory, backward_normer, backward_level, backward_passed = backward_summary
    identity = (
        jnp.zeros_like(forward_memory),
        jnp.zeros_like(forward_normer),
        jnp.full_like(forward_level, FLOOR_LEVEL),
        jnp.zeros_like(forward_passed),
    )
    forward_before = entering(
        (forward_memory, forward_normer, forward_level, forward_passed),
        "sp",
        join_states,
        identity,
        False,
    )
    backward_before = entering(
        (backward_memory, backward_normer, backward_level, backward_passed),
        "sp",
        join_states,
        identity,
        True,
    )
    zero_passed = jnp.zeros_like(start_level[0])
    forward_state = join_states(
        (start_memory[0], start_norm[0], start_level[0], zero_passed), forward_before
    )
    backward_state = join_states(
        (start_memory[1], start_norm[1], start_level[1], zero_passed), backward_before
    )
    forward_out = finish(forward_local, forward_state, queries)
    backward_out = jnp.flip(finish(backward_local, backward_state, flipped_queries), axis=1)
    both_ways = forward_out + backward_out
    both_ways = both_ways * lax.rsqrt(jnp.mean(both_ways * both_ways, axis=2, keepdims=True) + EPS)
    cell_out = (
        jnp.transpose(both_ways, (1, 0, 2)).reshape(rows_here, heads_here * value_width) * cell_gain
    ).astype(jnp.bfloat16)
    return lax.psum_scatter(
        (
            jnp.einsum("tc,dc->td", conv_out, conv_out_weight, preferred_element_type=jnp.float32)
            + jnp.einsum("tc,dc->td", cell_out, cell_out_weight, preferred_element_type=jnp.float32)
        ).astype(jnp.bfloat16),
        "tp",
        scatter_dimension=0,
        tiled=True,
    )


def solution(mesh):
    in_specs = (
        P("sp", None),
        P(),
        P("sp", "tp"),
        P("sp", "tp"),
        P(None, "tp"),
        P("tp"),
        P("tp"),
        P("sp", "tp"),
        P("sp", "tp"),
        P("sp", "tp"),
        P(),
        P(None, None, "tp", "sp"),
        P(None, "tp", None, None),
        P(None, "tp", None),
        P(None, "tp"),
        P("tp"),
        P("sp", "tp"),
        P("sp", "tp"),
    )
    out_specs = P(("sp", "tp"), None)
    return jax.shard_map(shards, mesh=mesh, in_specs=in_specs, out_specs=out_specs, check_vma=False)
```

profile of v0, /device:TPU:0, one launch (start us, length us, event | category | flops | bytes accessed | tf_op | source)
XLA Modules:
  0.0 1299.5 jit_solution(14842206472727980344)
XLA Ops:
  10.0 1.2 fusion.56
  11.2 1.4 fusion.176
  14.6 73.9 %all-gather.28.cloned.1.call-done = bf16[2048,1024]{1,0:T(8,128)(2,1)} async-done(((bf16[128,1024]{1,0:T(8,128)(2,1)}), bf16[2048,1024]{1,0:T(8,128)(2,1)}) %all-gather.28.cloned.1.call-update) | async-done | bytes 4194320 | tf_op jit(solution)/shard_map/all_gather | solution.py:172
  88.5 2.9 convolution_convert_fusion.2
  91.8 110.4 %all-gather.26.cloned.1.call-done = bf16[2048,2048]{1,0:T(8,128)(2,1)} async-done(((bf16[128,2048]{1,0:T(8,128)(2,1)}), bf16[2048,2048]{1,0:T(8,128)(2,1)}) %all-gather.26.cloned.1.call-update) | async-done | bytes 8388624 | tf_op jit(solution)/shard_map/all_gather | solution.py:173
  202.2 4.7 convolution_convert_fusion
  206.9 1.2 fusion.68
  208.1 6.8 rev.23
  214.9 3.4 convolution_add_fusion.1
  219.2 3.4 convolution_add_fusion.2
  224.3 39.2 %all-gather.20.cloned.1.call-done = bf16[2048,512]{1,0:T(8,128)(2,1)} async-done(((bf16[128,512]{1,0:T(8,128)(2,1)}), bf16[2048,512]{1,0:T(8,128)(2,1)}) %all-gather.20.cloned.1.call-update) | async-done | bytes 2097168 | tf_op jit(solution)/shard_map/all_gather | solution.py:169
  263.5 2.1 fusion.55
  265.6 59.7 %all-gather.22.cloned.1.call-done = bf16[2048,512]{1,0:T(8,128)(2,1)} async-done(((bf16[128,512]{1,0:T(8,128)(2,1)}), bf16[2048,512]{1,0:T(8,128)(2,1)}) %all-gather.22.cloned.1.call-update) | async-done | bytes 2097168 | tf_op jit(solution)/shard_map/all_gather | solution.py:170
  325.4 2.1 fusion.54
  327.5 3.2 collective-permute-start
  330.7 1.3 collective-permute-start.1
  333.7 41.2 %all-reduce.2 = (f32[64]{0:T(128)S(1)}, f32[64]{0:T(128)S(1)}) all-reduce(f32[64]{0:T(128)S(1)} %dynamic-update-slice.1, f32[64]{0:T(128)S(1)} %dynamic-update-slice), channel_id=5, replica_groups=mesh['sp'=16,'tp'=2] {'sp'}, use_global_device_ids=true, to_apply=%add.1 | all-reduce | flops 128 | bytes 1024
  375.1 36.5 %all-gather.8 = f32[16,1,4]{2,1,0:T(1,128)S(1)} all-gather(f32[1,1,4]{2,1,0:T(1,128)S(1)} %fusion.154), channel_id=1, replica_groups=mesh['sp'=16,'tp'=2] {'sp'}, dimensions={0}, use_global_device_ids=true | all-gather | bytes 272 | tf_op jit(solution)/shard_map/all_gather | solution.py:32
  411.7 38.8 %all-gather.6 = f32[16,1,4]{2,1,0:T(1,128)S(1)} all-gather(f32[1,1,4]{2,1,0:T(1,128)S(1)} %fusion.155), channel_id=1, replica_groups=mesh['sp'=16,'tp'=2] {'sp'}, dimensions={0}, use_global_device_ids=true | all-gather | bytes 272 | tf_op jit(solution)/shard_map/all_gather | solution.py:32
  450.5 1.8 fusion.180
  452.3 2.6 all-reduce.3
  455.5 2.9 convolution_convert_fusion.1
  458.5 0.9 fusion.82
  459.8 39.8 %all-gather.9 = f32[16,4,256]{2,1,0:T(4,128)} all-gather(f32[1,4,256]{2,1,0:T(4,128)S(1)} %fusion.136), channel_id=7, replica_groups=mesh['sp'=16,'tp'=2] {'sp'}, dimensions={0}, use_global_device_ids=true | all-gather | bytes 69632 | tf_op jit(solution)/shard_map/all_gather | solution.py:32
  500.1 39.8 %all-gather.7 = f32[16,4,256]{2,1,0:T(4,128)S(1)} all-gather(f32[1,4,256]{2,1,0:T(4,128)S(1)} %fusion.139), channel_id=4, replica_groups=mesh['sp'=16,'tp'=2] {'sp'}, dimensions={0}, use_global_device_ids=true | all-gather | bytes 69632 | tf_op jit(solution)/shard_map/all_gather | solution.py:32
  540.7 2.0 fusion.193
  542.7 1.7 fusion.194
  544.4 212.2 %all-gather.36.cloned.1.call-done = f32[64,512,256]{2,1,0:T(8,128)} async-done(((f32[4,512,256]{2,1,0:T(8,128)}), f32[64,512,256]{2,1,0:T(8,128)}) %all-gather.36.cloned.1.call-update) | async-done | bytes 33554448 | tf_op jit(solution)/shard_map/all_gather | solution.py:32
  756.7 50.9 %while.7 = (s32[]{:T(128)}, f32[4,512,256]{2,1,0:T(8,128)S(1)}, f32[4,256]{1,0:T(4,128)S(1)}, f32[4]{0:T(128)S(1)}, f32[4]{0:T(128)S(1)}, /*index=5*/s32[]{:T(12...) while((s32[]{:T(128)}, f32[4,512,256]{2,1,0:T(8,128)S(1)}, ...), condition=%wide.region_15.16_spmd, body=%wide.region_14.15_spmd.sunk | while | flops 1575962 | bytes 6304163 | solution.py:41
  756.8 2.6 fusion.221
  759.4 0.8 fusion.222
  760.2 2.6 fusion.221
  762.7 0.8 fusion.222
  763.5 2.6 fusion.221
  766.9 2.8 fusion.221
  770.6 2.6 fusion.221
  773.1 0.8 fusion.222
  774.0 2.6 fusion.221
  777.3 2.6 fusion.221
  779.9 0.8 fusion.222
  780.7 2.6 fusion.221
  784.1 2.6 fusion.221
  786.7 0.8 fusion.222
  787.5 2.6 fusion.221
  790.8 2.6 fusion.221
  794.2 2.6 fusion.221
  797.6 2.6 fusion.221
  800.9 2.6 fusion.221
  803.5 0.8 fusion.222
  804.3 2.6 fusion.221
  807.6 300.1 %all-gather.34.cloned.1.call-done = f32[64,512,256]{2,1,0:T(8,128)} async-done(((f32[4,512,256]{2,1,0:T(8,128)}), f32[64,512,256]{2,1,0:T(8,128)}) %all-gather.34.cloned.1.call-update) | async-done | bytes 33554448 | tf_op jit(solution)/shard_map/all_gather | solution.py:32
  1107.8 1.5 broadcast.304.clone
  1109.3 0.8 subtract_exponential_fusion.11
  1110.2 0.8 fusion.138
  1111.9 1.0 convolution_multiply_fusion.1
  1112.9 1.1 fusion.38
  1114.1 3.5 fusion.39
  1117.6 6.9 rev.26
  1126.1 3.3 multiply_reduce_fusion
  1130.5 90.5 %all-gather.32.cloned.1.call-done = bf16[2048,2048]{1,0:T(8,128)(2,1)} async-done(((bf16[128,2048]{1,0:T(8,128)(2,1)}), bf16[2048,2048]{1,0:T(8,128)(2,1)}) %all-gather.32.cloned.1.call-update) | async-done | bytes 8388624 | tf_op jit(solution)/shard_map/all_gather | solution.py:183
  1221.1 6.3 fusion.195
  1227.4 55.1 %all-gather.24.cloned.1.call-done = bf16[2048,512]{1,0:T(8,128)(2,1)} async-done(((bf16[128,512]{1,0:T(8,128)(2,1)}), bf16[2048,512]{1,0:T(8,128)(2,1)}) %all-gather.24.cloned.1.call-update) | async-done | bytes 2097168 | tf_op jit(solution)/shard_map/all_gather | solution.py:182
  1282.5 3.2 fusion.14
  1285.8 6.9 reduce-scatter.2.cloned.1.call-done
  (172 shorter events, 22.7 us)
Async XLA Ops:
  6.5 4.7 copy-start
  6.5 82.0 %copy-start.3 = (bf16[128,2048]{1,0:T(8,128)(2,1)S(1)}, bf16[128,2048]{1,0:T(8,128)(2,1)}, u32[]{:S(2)}) copy-start(bf16[128,2048]{1,0:T(8,128)(2,1)} %param.22) | copy-start | bytes 1572868
  6.5 82.0 %copy-start.9 = (f32[2048]{0:T(1024)S(1)}, f32[2048]{0:T(1024)}, u32[]{:S(2)}) copy-start(f32[2048]{0:T(1024)} %param.23) | copy-start | bytes 24580
  6.5 6.1 copy-start.15
  6.5 82.0 %all-gather.28.cloned.1.call-start = ((), (), s32[]{:S(2)}) async-start(), calls=%async_computation.5 | async-start | bytes 4456448 | tf_op jit(solution)/shard_map/all_gather | solution.py:172
  7.3 194.9 %all-gather.26.cloned.1.call-start = ((), (), s32[]{:S(2)}) async-start(), calls=%async_computation.4 | async-start | bytes 8912896 | tf_op jit(solution)/shard_map/all_gather | solution.py:173
  8.0 255.5 %all-gather.20.cloned.1.call-start = ((), (), s32[]{:S(2)}) async-start(), calls=%async_computation.1 | async-start | bytes 2228224 | tf_op jit(solution)/shard_map/all_gather | solution.py:169
  8.8 316.6 %all-gather.22.cloned.1.call-start = ((), (), s32[]{:S(2)}) async-start(), calls=%async_computation.2 | async-start | bytes 2228224 | tf_op jit(solution)/shard_map/all_gather | solution.py:170
  9.3 446.2 %all-gather.30.cloned.1.call-start = ((), (), s32[]{:S(2)}) async-start(), calls=%async_computation.6 | async-start | bytes 4456448 | tf_op jit(solution)/shard_map/all_gather | solution.py:171
  9.9 746.6 %all-gather.36.cloned.1.call-start = ((), (), s32[]{:S(2)}) async-start(), calls=%async_computation.10 | async-start | bytes 35651584 | tf_op jit(solution)/shard_map/all_gather | solution.py:32
  214.9 3.4 copy-start.4
  218.4 889.4 %all-gather.34.cloned.1.call-start = ((), (), s32[]{:S(2)}) async-start(), calls=%async_computation.9 | async-start | bytes 35651584 | tf_op jit(solution)/shard_map/all_gather | solution.py:32
  222.6 1.6 copy-start.11
  222.6 998.4 %all-gather.32.cloned.1.call-start = ((), (), s32[]{:S(2)}) async-start(), calls=%async_computation.7 | async-start | bytes 8912896 | tf_op jit(solution)/shard_map/all_gather | solution.py:183
  223.4 1059.1 %all-gather.24.cloned.1.call-start = ((), (), s32[]{:S(2)}) async-start(), calls=%async_computation.3 | async-start | bytes 2228224 | tf_op jit(solution)/shard_map/all_gather | solution.py:182
  224.1 1068.5 %reduce-scatter.2.cloned.1.call-start = ((), (), s32[]{:S(2)}) async-start(), calls=%async_computation.8 | async-start | bytes 786432 | tf_op jit(solution)/shard_map/reduce_scatter | solution.py:271
  265.6 66.4 %copy-start.21 = (u32[32]{0:T(128)S(1)}, u32[32]{0:T(128)}, u32[]{:S(2)}) copy-start(u32[32]{0:T(128)} %constant.147) | copy-start | bytes 388
  265.6 184.9 %copy-start.16 = (f32[512]{0:T(512)S(1)}, f32[512]{0:T(512)}, u32[]{:S(2)}) copy-start(f32[512]{0:T(512)} %param.27) | copy-start | bytes 6148
  327.5 122.9 %collective-permute-start = (bf16[15,512]{1,0:T(8,128)(2,1)S(1)}, bf16[15,512]{1,0:T(8,128)(2,1)S(1)}, u32[]{:S(2)}, u32[]{:S(2)}) collective-permute-start(bf16[15,512]{1,0:T(8,128)(2,1)S(1)} %get-tuple-element.417), channel_id=1, source_target_pairs={{0,2},{2,4},{4,6},{6,8},{8,10},{10,12},{12,14},{14,16},{16,18},{18... | collective-permute-start | bytes 46088 | tf_op jit(solution)/shard_map/ppermute | solution.py:22
  330.7 119.7 %collective-permute-start.1 = (bf16[15,512]{1,0:T(8,128)(2,1)S(1)}, bf16[15,512]{1,0:T(8,128)(2,1)S(1)}, u32[]{:S(2)}, u32[]{:S(2)}) collective-permute-start(bf16[15,512]{1,0:T(8,128)(2,1)S(1)} %get-tuple-element.418), channel_id=1, source_target_pairs={{2,0},{4,2},{6,4},{8,6},{10,8},{12,10},{14,12},{16,14},{18,16},{20... | collective-permute-start | bytes 46088 | tf_op jit(solution)/shard_map/ppermute | solution.py:23
  1109.3 2.5 copy-start.13
  1109.3 2.5 copy-start.14
  1109.3 2.5 copy-start.20
  1109.3 3.6 copy-start.5
  1109.3 3.6 copy-start.8
  1111.9 2.2 copy-start.6
  1117.6 7.5 copy-start.10
  1124.5 1.6 copy-start.2
  1129.4 0.7 copy-start.12
  1130.5 152.0 %copy-start.7 = (f32[128,512]{1,0:T(8,128)S(1)}, f32[128,512]{1,0:T(8,128)}, u32[]{:S(2)}) copy-start(f32[128,512]{1,0:T(8,128)} %get-tuple-element.402) | copy-start | bytes 786436
  1130.5 152.0 %copy-start.17 = (f32[512]{0:T(512)S(1)}, f32[512]{0:T(512)}, u32[]{:S(2)}) copy-start(f32[512]{0:T(512)} %param.28) | copy-start | bytes 6148
  1130.5 152.0 %copy-start.18 = (f32[128]{0:T(128)S(1)}, f32[128]{0:T(128)}, u32[]{:S(2)}) copy-start(f32[128]{0:T(128)} %get-tuple-element.462) | copy-start | bytes 1540
  1130.5 152.0 %copy-start.19 = (f32[128]{0:T(128)S(1)}, f32[128]{0:T(128)}, u32[]{:S(2)}) copy-start(f32[128]{0:T(128)} %get-tuple-element.463) | copy-start | bytes 1540
  1282.5 10.2 copy-start.1
Sparse Core Ops, SparseCore 0:
  10.1 78.3 all-gather.27
  91.3 110.8 all-gather.25
  205.0 58.4 all-gather.19
  266.1 59.1 all-gather.21
  328.0 74.8 all-gather.29
  405.5 350.9 all-gather.35
  759.3 348.4 all-gather.33
  1110.5 110.4 all-gather.31
  1223.8 58.6 all-gather.23
  1285.9 6.7 reduce-scatter.1
where the time goes:
time: 1300 us
  waiting for transfers between devices  953 us (73%)
  blocking collectives  199 us (15%)
  other arithmetic  60 us (5%)
  matrix products  49.3 us (4%)
  local copies, waits for them, and re-layouts  19 us (1%)
  between operations  14.7 us (1%)
    all_gather x2, waiting for transfers between devices, entering(): gathered = jax.tree.map(lambda a: lax.all_gather(a, axis), part)  512 us
    all_gather x4, blocking collectives, entering(): gathered = jax.tree.map(lambda a: lax.all_gather(a, axis), part)  155 us
    all_gather x1, waiting for transfers between devices, shards(): lax.all_gather(value_weight, 'sp', axis=0, tiled=True)  110 us
    all_gather x1, waiting for transfers between devices, shards(): lax.all_gather(out_cell_weight, 'sp', axis=0, tiled=True)  90.5 us
    all_gather x1, waiting for transfers between devices, shards(): lax.all_gather(key_weight, 'sp', axis=0, tiled=True)  73.9 us
    all_gather x1, waiting for transfers between devices, shards(): lax.all_gather(conv_gate_weight, 'sp', axis=0, tiled=True)  59.7 us
    all_gather x1, waiting for transfers between devices, shards(): lax.all_gather(out_conv_weight, 'sp', axis=0, tiled=True)  55.1 us
    unnamed x1, blocking collectives  41.2 us
  transfers between devices with their start and end apart: 12, of which 9 were waited for; matrix products, arithmetic and copies ran while one was open for 10% of the time, Pallas kernels for 0%

commit v1 on v0

v1 whole, which is shorter than its diff:
```python
import jax
import jax.numpy as jnp
from jax import lax
from jax.sharding import Mesh, PartitionSpec as P

EPS = 1e-06
HIGHEST = lax.Precision.HIGHEST
CHUNK = 128
OUTER, HEAD, TP = "outer", "head", "tp"


def running_sum(values):
    lead, length = values.shape[:-1], values.shape[-1]
    chunk = min(CHUNK, length)
    count = length // chunk
    blocks = values.reshape(lead + (count, chunk))
    inside = (jnp.arange(chunk)[:, None] <= jnp.arange(chunk)[None, :]).astype(jnp.float32)
    before = (jnp.arange(count)[:, None] < jnp.arange(count)[None, :]).astype(jnp.float32)
    local = jnp.einsum("...cs,st->...ct", blocks, inside, precision=HIGHEST)
    start = jnp.einsum("...c,cd->...d", local[..., -1], before, precision=HIGHEST)
    return (local + start[..., None]).reshape(values.shape)


def own_columns(weight, parts, part):
    return lax.dynamic_slice_in_dim(
        weight, part * (weight.shape[-1] // parts), weight.shape[-1] // parts, weight.ndim - 1
    )


def by_head(weights, parts):
    return jnp.concatenate(
        [
            jnp.transpose(w.reshape(w.shape[0], parts, w.shape[1] // parts), (1, 0, 2))
            for w in weights
        ],
        axis=2,
    )


def spread(blocks):
    mine = lax.all_to_all(blocks, HEAD, 0, 0, tiled=True)
    return mine.reshape(mine.shape[0] * mine.shape[1], mine.shape[2])


def shards(
    tokens,
    norm_gain,
    conv_value_weight,
    conv_gate_weight,
    conv_kernel,
    conv_bias,
    channel_gain,
    query_weight,
    key_weight,
    value_weight,
    gate_weight,
    gate_offset,
    start_memory,
    start_norm,
    start_level,
    cell_gain,
    out_conv_weight,
    out_cell_weight,
):
    parts = lax.axis_size(HEAD)
    groups = lax.axis_size(OUTER)
    group = lax.axis_index(OUTER)
    part = lax.axis_index(HEAD)
    key_width = start_norm.shape[2]
    value_width = start_memory.shape[2]
    all_channels = conv_bias.shape[0] * lax.axis_size(TP)
    heads_here = start_level.shape[1]
    channels = conv_bias.shape[0] // parts

    features = tokens.astype(jnp.float32)
    normed = (
        features * lax.rsqrt(jnp.mean(features * features, axis=1, keepdims=True) + EPS) * norm_gain
    ).astype(jnp.bfloat16)

    gate_pre = jnp.dot(normed, gate_weight, preferred_element_type=jnp.float32)
    gate_pre = gate_pre.reshape(gate_pre.shape[0], 2, 2, gate_weight.shape[1] // 4)
    gate_pre = lax.dynamic_slice_in_dim(gate_pre, lax.axis_index(TP) * heads_here, heads_here, 3)
    gate_pre = jnp.transpose(gate_pre, (1, 2, 3, 0)) + gate_offset
    gates = lax.all_gather(gate_pre, (OUTER, HEAD), axis=3, tiled=True)
    gates = lax.dynamic_index_in_dim(gates, part, 2, False)

    rows = lax.all_gather(normed, HEAD, axis=0, tiled=True)
    here = rows.shape[0]

    key_value_part = lax.all_gather(
        spread(by_head((key_weight, value_weight), parts)), OUTER, axis=0, tiled=True
    )
    other_part = lax.all_gather(
        spread(by_head((conv_value_weight, conv_gate_weight, query_weight), parts)),
        OUTER,
        axis=0,
        tiled=True,
    )
    out_part = lax.all_gather(
        spread(by_head((out_conv_weight, out_cell_weight), parts)), OUTER, axis=0, tiled=True
    )

    key_value = jnp.dot(rows, key_value_part, preferred_element_type=jnp.float32).astype(
        jnp.bfloat16
    )
    all_key_value = lax.all_gather(key_value, OUTER, axis=0, tiled=True)

    others = jnp.dot(rows, other_part, preferred_element_type=jnp.float32).astype(jnp.bfloat16)
    queries = others[:, 2 * channels :]

    gated = (
        others[:, :channels].astype(jnp.float32)
        * jax.nn.sigmoid(others[:, channels : 2 * channels].astype(jnp.float32))
    ).astype(jnp.bfloat16)
    reach = conv_kernel.shape[0] // 2
    up = [(i, i + 1) for i in range(groups - 1)]
    down = [(j, i) for i, j in up]
    before = lax.ppermute(gated[here - reach :], OUTER, up)
    after = lax.ppermute(gated[:reach], OUTER, down)
    padded = jnp.concatenate([before, gated, after], axis=0).astype(jnp.float32)
    taps = own_columns(conv_kernel, parts, part)
    conv_sum = own_columns(conv_bias, parts, part) + sum(
        taps[offset] * padded[offset : offset + here] for offset in range(conv_kernel.shape[0])
    )
    stats = lax.psum(
        jnp.stack([jnp.sum(conv_sum, axis=1), jnp.sum(conv_sum * conv_sum, axis=1)]), (HEAD, TP)
    )
    channel_mean = stats[0] / all_channels
    channel_var = stats[1] / all_channels - channel_mean * channel_mean
    conv_out = jax.nn.silu(
        (conv_sum - channel_mean[:, None])
        * lax.rsqrt(channel_var + EPS)[:, None]
        * own_columns(channel_gain, parts, part)
    ).astype(jnp.bfloat16)

    total = gates.shape[2]
    in_gate = gates[:, 0]
    log_forget = jax.nn.log_sigmoid(gates[:, 1])
    whole = jnp.round(log_forget)
    both = jnp.stack([whole, log_forget - whole])
    both = jnp.stack([both[:, 0], jnp.flip(both[:, 1], axis=1)], axis=1)
    both = running_sum(both)
    passed = jnp.stack([both[:, 0], jnp.flip(both[:, 1], axis=1)], axis=1)
    passed_here = lax.dynamic_slice_in_dim(passed, group * here, here, 2)
    keys = all_key_value[:, :key_width]
    values = all_key_value[:, key_width:]
    products = lax.dot_general(
        queries, keys, (((1,), (1,)), ((), ())), preferred_element_type=jnp.float32
    ) * (key_width**-0.5)
    at_row = (group * here + jnp.arange(here))[:, None]
    at_column = jnp.arange(total)[None, :]
    levels = lax.dynamic_index_in_dim(start_level, part, 1, False)
    norms = lax.dynamic_index_in_dim(start_norm, part, 1, False)
    memories = lax.dynamic_index_in_dim(start_memory, part, 1, False)
    wide_queries = queries.astype(jnp.float32)
    scaled = 0.0
    entered = 0.0
    for way in range(2):
        row_whole, row_rest = passed_here[0, way], passed_here[1, way]
        table = (row_whole[:, None] - passed[0, way][None, :]) + (
            row_rest[:, None] + (in_gate[way] - passed[1, way])[None, :]
        )
        seen = at_column <= at_row if way == 0 else at_column >= at_row
        table = jnp.where(seen, table, -jnp.inf)
        start = row_whole + row_rest + levels[way]
        top = jnp.maximum(start, jnp.max(table, axis=1))
        scores = products * jnp.exp(table - top[:, None])
        entry = jnp.exp(start - top)
        denominator = jnp.sum(scores, axis=1) + entry * jnp.sum(
            wide_queries * norms[way][None, :], axis=1
        )
        inverse = 1.0 / jnp.maximum(jnp.abs(denominator), 1.0)
        scaled = scaled + scores * inverse[:, None]
        entered = entered + (entry * inverse)[:, None] * lax.dot_general(
            queries,
            memories[way].astype(jnp.bfloat16),
            (((1,), (1,)), ((), ())),
            preferred_element_type=jnp.float32,
        )
    both_ways = entered + jnp.dot(
        scaled.astype(jnp.bfloat16), values, preferred_element_type=jnp.float32
    )
    both_ways = both_ways * lax.rsqrt(jnp.mean(both_ways * both_ways, axis=1, keepdims=True) + EPS)
    cell_out = (both_ways * own_columns(cell_gain, parts, part)).astype(jnp.bfloat16)

    partial = lax.dot_general(
        jnp.concatenate([conv_out, cell_out], axis=1),
        out_part,
        (((1,), (1,)), ((), ())),
        preferred_element_type=jnp.float32,
    ).astype(jnp.bfloat16)
    return lax.psum_scatter(partial, (HEAD, TP), scatter_dimension=0, tiled=True)


def solution(mesh):
    split = (OUTER, HEAD)
    in_specs = (
        P(split, None),
        P(),
        P(split, TP),
        P(split, TP),
        P(None, TP),
        P(TP),
        P(TP),
        P(split, TP),
        P(split, TP),
        P(split, TP),
        P(),
        P(None, None, TP, split),
        P(None, TP, None, None),
        P(None, TP, None),
        P(None, TP),
        P(TP),
        P(split, TP),
        P(split, TP),
    )
    out_specs = P((OUTER, HEAD, TP), None)

    def run(*arrays):
        sequence, tensor = mesh.shape["sp"], mesh.shape["tp"]
        heads = arrays[14].shape[1] // tensor
        parts = heads if sequence % heads == 0 else 1
        assert parts == heads
        fine = Mesh(mesh.devices.reshape(sequence // parts, parts, tensor), (OUTER, HEAD, TP))
        return jax.shard_map(
            shards, mesh=fine, in_specs=in_specs, out_specs=out_specs, check_vma=False
        )(*arrays)

    return run
```

time: 1300 us -> 342 us (0.26)
  waiting for transfers between devices: 953 us -> 172 us
  blocking collectives: 199 us -> 93.9 us
  other arithmetic: 60 us -> 10 us
  matrix products: 49.3 us -> 24.4 us
    all_gather x9 -> x5, waiting for transfers between devices: 941 us -> 128 us  [the longest x1 44.4 us: shards(): lax.all_gather(spread(by_head((out_conv_weight, out_cell_weight), parts))...]
    all_gather x4 -> x1, blocking collectives: 155 us -> 44.4 us  [shards(): gates = lax.all_gather(gate_pre, (OUTER, HEAD), axis=3, tiled=True)]
    add x31 -> x2, other arithmetic: 51.1 us -> 0.08 us  [the longest x1 0.08 us: running_sum(): return (local + start[..., None]).reshape(values.shape)]
    unnamed x1 -> x0, blocking collectives: 41.2 us -> none
    all_to_all x0 -> x2, blocking collectives: none -> 36.7 us  [spread(): mine = lax.all_to_all(blocks, HEAD, 0, 0, tiled=True)]
    reduce_scatter x1, waiting for transfers between devices: 6.88 us -> 40 us  [shards(): lax.psum_scatter(partial, (HEAD, TP), scatter_dimension=0, tiled=True)]
    dot_general x23 -> x9, matrix products: 47.9 us -> 24.1 us  [the longest x1 5.21 us: shards(): jnp.dot(rows, key_value_part, preferred_element_type=jnp.float32)]
  transfers between devices with their start and end apart: 12 -> 9, of which waited for: 9 -> 6; matrix products, arithmetic and copies ran while one was open for 10% -> 13% of each run, Pallas kernels for 0% -> 0%
where the time goes in v1:
time: 342 us; the launch traced here: 341 us
  waiting for transfers between devices  172 us (50%)
  blocking collectives  93.9 us (27%)
  matrix products  24.4 us (7%)
  local copies, waits for them, and re-layouts  19.7 us (6%)
  between operations  13.9 us (4%)
  other arithmetic  10 us (3%)
  starting transfers between devices  7.07 us (2%)
    all_gather x1, waiting for transfers between devices, shards(): lax.all_gather(spread(by_head((out_conv_weight, out_cell_weight), parts))...  44.4 us
    all_gather x1, blocking collectives, shards(): gates = lax.all_gather(gate_pre, (OUTER, HEAD), axis=3, tiled=True)  44.4 us
    reduce_scatter x1, waiting for transfers between devices, shards(): lax.psum_scatter(partial, (HEAD, TP), scatter_dimension=0, tiled=True)  40 us
    all_gather x1, waiting for transfers between devices, shards(): all_key_value = lax.all_gather(key_value, OUTER, axis=0, tiled=True)  38.1 us
    all_to_all x2, blocking collectives, spread(): mine = lax.all_to_all(blocks, HEAD, 0, 0, tiled=True)  36.7 us
    all_gather x1, waiting for transfers between devices, shards(): lax.all_gather(spread(by_head((key_weight, value_weight), parts)), OUTER,...  22.9 us
    all_gather x1, waiting for transfers between devices, shards(): lax.all_gather(spread(by_head((conv_value_weight, conv_gate_weight, query...  22.5 us
    psum x1, blocking collectives, shards(): lax.psum(jnp.stack([jnp.sum(conv_sum, axis=1), jnp.sum(conv_sum * conv_su...  12.8 us
  transfers between devices with their start and end apart: 9, of which 6 were waited for; matrix products, arithmetic and copies ran while one was open for 13% of the time, Pallas kernels for 0%

profile of v1, /device:TPU:0, one launch (start us, length us, event | category | flops | bytes accessed | tf_op | source)
XLA Modules:
  0.0 341.1 jit_solution(2776447201779496806)
XLA Ops:
  6.5 1.3 fusion.8
  7.8 2.1 fusion.10
  9.9 0.0 all-gather.10.cloned.1.call-start
  10.0 1.4 copy.29
  11.3 1.1 copy.28
  12.5 0.1 pad_maximum_fusion
  12.5 22.1 %all_to_all.15 = bf16[4,128,768]{1,2,0:T(8,128)(2,1)S(1)} all-to-all(bf16[4,128,768]{1,2,0:T(8,128)(2,1)S(1)} %pad_maximum_fusion), channel_id=1, replica_groups=mesh['outer'=4,'head'=4,'tp'=2] {'head'}, dimensions={0} | all-to-all | bytes 1572864 | tf_op jit(solution)/shard_map/all_to_all | solution.py:41
  34.6 1.2 copy.30
  35.9 0.2 copy.25
  36.1 0.1 copy.23
  36.2 0.1 copy.24
  36.4 14.6 %all_to_all.16 = bf16[4,128,512]{1,2,0:T(8,128)(2,1)S(1)} all-to-all(bf16[4,128,512]{1,2,0:T(8,128)(2,1)S(1)} %pad_maximum_fusion.2), channel_id=1, replica_groups=mesh['outer'=4,'head'=4,'tp'=2] {'head'}, dimensions={0} | all-to-all | bytes 1048576 | tf_op jit(solution)/shard_map/all_to_all | solution.py:41
  51.0 1.0 copy.26
  52.0 0.3 copy.33
  52.3 0.1 copy.32
  52.4 0.9 pad_maximum_fusion.1
  53.3 3.5 %all-to-all-start.2 = ((bf16[4,128,640]{1,2,0:T(8,128)(2,1)}), bf16[4,128,640]{1,2,0:T(8,128)(2,1)S(1)}, u32[]{:S(2)}, u32[]{:S(2)}) async-start(bf16[4,128,640]{1,2,0:T(8,128)(2,1)} %pad_maximum_fusion.1), calls=%async_computation.2 | async-start | bytes 1310720 | tf_op jit(solution)/shard_map/all_to_all | solution.py:41
  56.8 0.0 all-gather.12.cloned.1.call-start
  56.9 0.3 fusion.85
  57.2 44.4 %all_gather.20 = f32[2,2,4,2048]{3,2,1,0:T(4,128)S(1)} all-gather(f32[2,2,4,128]{3,2,1,0:T(4,128)S(1)} %bitcast_add_fusion), channel_id=1, replica_groups=mesh['outer'=4,'head'=4,'tp'=2] {'outer','head'}, dimensions={3}, use_global_device_ids=true | all-gather | bytes 139264 | tf_op jit(solution)/shard_map/all_gather | solution.py:84
  101.6 0.1 fusion.79
  101.8 22.9 %all-gather.10.cloned.1.call-done = bf16[2048,768]{1,0:T(8,128)(2,1)} async-done(((bf16[512,768]{1,0:T(8,128)(2,1)}), bf16[2048,768]{1,0:T(8,128)(2,1)}) %all-gather.10.cloned.1.call-update) | async-done | bytes 3145744 | tf_op jit(solution)/shard_map/all_gather | solution.py:90
  124.7 5.2 %convolution_convert_fusion.1 = bf16[512,768]{1,0:T(8,128)(2,1)} fusion(bf16[512,2048]{1,0:T(8,128)(2,1)} %all-gather.6.cloned.1.call-done, bf16[2048,768]{1,0:T(8,128)(2,1)} %all-gather.10.cloned.1.call-done), kind=kOutput, calls=%fused_computation.14 | convolution fusion | flops 1611005952 | bytes 6029312 | tf_op jit(solution)/shard_map/dot_general | solution.py:103
  130.0 1.4 rev.7
  131.4 0.2 fusion.53
  131.6 0.2 slice_reduce_fusion
  131.8 0.1 fusion.66
  131.9 0.1 broadcast_add_fusion
  132.1 1.4 slice.403
  133.5 1.4 rev.8
  135.0 1.4 slice.399
  136.4 0.1 constant_dynamic-slice_fusion.2
  136.5 0.5 fusion.84
  137.0 1.0 dynamic-slice_bitcast_fusion.29
  138.0 1.1 fusion.70
  139.2 1.3 dynamic-slice_convert_fusion
  140.5 2.4 fusion.1
  142.9 0.7 constant_dynamic-slice_fusion.1
  143.6 0.8 dynamic_slice.34
  144.3 0.8 dynamic_slice.36
  145.1 0.8 dynamic_slice.43
  145.8 0.6 fusion.78
  146.5 0.6 fusion.77
  147.1 1.1 copy.34
  148.3 22.5 %all-gather.8.cloned.1.call-done = bf16[2048,512]{1,0:T(8,128)(2,1)} async-done(((bf16[512,512]{1,0:T(8,128)(2,1)}), bf16[2048,512]{1,0:T(8,128)(2,1)}) %all-gather.8.cloned.1.call-update) | async-done | bytes 2097168 | tf_op jit(solution)/shard_map/all_gather | solution.py:93
  170.8 3.5 %convolution_convert_fusion.2 = bf16[512,512]{1,0:T(8,128)(2,1)S(1)} fusion(bf16[512,2048]{1,0:T(8,128)(2,1)} %all-gather.6.cloned.1.call-done, bf16[2048,512]{1,0:T(8,128)(2,1)} %all-gather.8.cloned.1.call-done), kind=kOutput, calls=%fused_computation.21 | convolution fusion | flops 1074003968 | bytes 4718592 | tf_op jit(solution)/shard_map/dot_general | solution.py:108
  174.3 0.1 multiply_convert_fusion.2
  174.4 2.1 collective-permute-start
  176.5 1.3 collective-permute-start.1
  177.8 0.2 fusion.16
  178.0 4.0 %collective-permute-done.1 = bf16[15,128]{1,0:T(8,128)(2,1)S(1)} collective-permute-done((bf16[15,128]{1,0:T(8,128)(2,1)S(1)}, bf16[15,128]{1,0:T(8,128)(2,1)S(1)}, u32[]{:S(2)}, u32[]{:S(2)}) %collective-permute-start.1) | collective-permute-done | bytes 3872 | tf_op jit(solution)/shard_map/ppermute | solution.py:119
  182.0 1.1 fusion.75
  183.1 12.8 %psum.7 = f32[2,512]{1,0:T(2,128)S(1)} all-reduce(f32[2,512]{1,0:T(2,128)S(1)} %pad_maximum_fusion.4), channel_id=1, replica_groups=mesh['outer'=4,'head'=4,'tp'=2] {'head','tp'}, use_global_device_ids=true, to_apply=%region_3.4 | all-reduce | flops 1024 | bytes 8192 | tf_op jit(solution)/shard_map/psum | solution.py:125
  196.0 0.2 multiply_convert_fusion.1
  196.2 0.1 copy.31
  196.3 38.1 %all-gather.12.cloned.1.call-done = bf16[2048,768]{1,0:T(8,128)(2,1)} async-done(((bf16[512,768]{1,0:T(8,128)(2,1)}), bf16[2048,768]{1,0:T(8,128)(2,1)}) %all-gather.12.cloned.1.call-update) | async-done | bytes 3145744 | tf_op jit(solution)/shard_map/all_gather | solution.py:106
  234.5 5.0 %fusion.73 = (f32[512]{0:T(512)S(1)}, f32[512]{0:T(512)S(1)}, f32[512,2048]{1,0:T(8,128)S(1)}) fusion(f32[512]{0:T(512)S(1)} %get-tuple-element.20, f32[2048]{0:T(1024)S(1)} %bitcast.182, f32[512]{0:T(512)S(1)} %bitcast.201, f32[2048]{0:T(1024)S(1)} %bitcast.185, f32[512]{0:T(512)S(1)} %bitcast.205, s32[512]{0:T(512)S(1)} %iota_add_fusion, ...), kind=kOutput, calls=%fused_computation.199 | convolution fusion | flops 554695680 | bytes 5556224 | tf_op jit(solution)/shard_map/dot_general | solution.py:147
  239.5 0.3 convolution_multiply_fusion.1
  239.8 4.5 %fusion.2 = f32[512,512]{0,1:T(8,128)S(1)} fusion(bf16[2048,768]{1,0:T(8,128)(2,1)S(1)} %copy-done.9, f32[512]{0:T(512)S(1)} %get-tuple-element.15, f32[512]{0:T(512)S(1)} %get-tuple-element.17, f32[512,2048]{1,0:T(8,128)S(1)} %get-tuple-element.75, f32[512]{0:T(512)S(1)} %get-tuple-element.20, f32[2048]{0:T(1024)S(1)} %bitcast.183, f32[512]{0:T(512)S(1)} %bitcast.202, ...), kind=kOutput, calls=%fused_computation.10 | convolution fusion | flops 1093664768 | bytes 7391232 | tf_op jit(solution)/shard_map/dot_general | solution.py:180
  244.3 0.4 multiply_reduce_fusion
  244.7 0.2 multiply_convert_fusion
  244.9 44.4 %all-gather.14.cloned.1.call-done = bf16[2048,640]{1,0:T(8,128)(2,1)} async-done(((bf16[512,640]{1,0:T(8,128)(2,1)}), bf16[2048,640]{1,0:T(8,128)(2,1)}) %all-gather.14.cloned.1.call-update) | async-done | bytes 2621456 | tf_op jit(solution)/shard_map/all_gather | solution.py:99
  289.3 4.9 %convolution_convert_fusion = bf16[512,2048]{1,0:T(8,128)(2,1)} fusion(bf16[2048,640]{1,0:T(8,128)(2,1)} %all-gather.14.cloned.1.call-done, bf16[512,512]{0,1:T(8,128)(2,1)S(1)} %multiply_convert_fusion, bf16[512,128]{0,1:T(8,128)(2,1)S(1)} %copy.31), kind=kOutput, calls=%fused_computation.9 | convolution fusion | flops 1344536576 | bytes 5373952 | tf_op jit(solution)/shard_map/dot_general | solution.py:186
  294.2 40.0 %reduce-scatter.2.cloned.1.call-done = bf16[64,2048]{1,0:T(8,128)(2,1)} async-done(((bf16[512,2048]{1,0:T(8,128)(2,1)}), bf16[64,2048]{1,0:T(8,128)(2,1)}) %reduce-scatter.2.cloned.1.call-update) | async-done | bytes 262160 | tf_op jit(solution)/shard_map/reduce_scatter | solution.py:192
  (58 shorter events, 0.7 us)
Async XLA Ops:
  6.5 50.3 %copy-start = (bf16[2048,32]{0,1:T(8,128)(2,1)S(1)}, bf16[2048,32]{0,1:T(8,128)(2,1)}, u32[]{:S(2)}) copy-start(bf16[2048,32]{0,1:T(8,128)(2,1)} %param.28) | copy-start | bytes 393220
  6.5 95.2 %all-gather.6.cloned.1.call-start = ((), (), s32[]{:S(2)}) async-start(), calls=%async_computation.4 | async-start | bytes 2621440 | tf_op jit(solution)/shard_map/all_gather | solution.py:87
  7.8 28.1 %copy-start.3 = (bf16[128,1024]{1,0:T(8,128)(2,1)S(1)}, bf16[128,1024]{1,0:T(8,128)(2,1)}, u32[]{:S(2)}) copy-start(bf16[128,1024]{1,0:T(8,128)(2,1)} %param.25) | copy-start | bytes 786436
  9.9 26.2 %copy-start.4 = (bf16[128,512]{1,0:T(8,128)(2,1)S(1)}, bf16[128,512]{1,0:T(8,128)(2,1)}, u32[]{:S(2)}) copy-start(bf16[128,512]{1,0:T(8,128)(2,1)} %param.20) | copy-start | bytes 393220
  9.9 26.3 %copy-start.5 = (bf16[128,512]{1,0:T(8,128)(2,1)S(1)}, bf16[128,512]{1,0:T(8,128)(2,1)}, u32[]{:S(2)}) copy-start(bf16[128,512]{1,0:T(8,128)(2,1)} %param.21) | copy-start | bytes 393220
  9.9 114.7 %all-gather.10.cloned.1.call-start = ((), (), s32[]{:S(2)}) async-start(), calls=%async_computation.6 | async-start | bytes 3932160 | tf_op jit(solution)/shard_map/all_gather | solution.py:90
  12.5 39.5 %copy-start.2 = (bf16[128,2048]{1,0:T(8,128)(2,1)S(1)}, bf16[128,2048]{1,0:T(8,128)(2,1)}, u32[]{:S(2)}) copy-start(bf16[128,2048]{1,0:T(8,128)(2,1)} %param.35) | copy-start | bytes 1572868
  34.6 17.7 %copy-start.6 = (bf16[128,512]{1,0:T(8,128)(2,1)S(1)}, bf16[128,512]{1,0:T(8,128)(2,1)}, u32[]{:S(2)}) copy-start(bf16[128,512]{1,0:T(8,128)(2,1)} %param.34) | copy-start | bytes 393220
  35.8 135.0 %all-gather.8.cloned.1.call-start = ((), (), s32[]{:S(2)}) async-start(), calls=%async_computation.5 | async-start | bytes 2621440 | tf_op jit(solution)/shard_map/all_gather | solution.py:93
  36.1 20.8 %copy-start.1 = (bf16[128,2048]{1,0:T(8,128)(2,1)S(1)}, bf16[128,2048]{1,0:T(8,128)(2,1)}, u32[]{:S(2)}) copy-start(bf16[128,2048]{1,0:T(8,128)(2,1)} %fusion.10) | copy-start | bytes 1572868
  36.3 20.9 %copy-start.7 = (f32[2,2,4,128]{3,2,1,0:T(4,128)S(1)}, f32[2,2,4,128]{3,2,1,0:T(4,128)}, u32[]{:S(2)}) copy-start(f32[2,2,4,128]{3,2,1,0:T(4,128)} %param.29) | copy-start | bytes 24580
  53.3 93.7 %all-to-all-start.2 = ((bf16[4,128,640]{1,2,0:T(8,128)(2,1)}), bf16[4,128,640]{1,2,0:T(8,128)(2,1)S(1)}, u32[]{:S(2)}, u32[]{:S(2)}) async-start(bf16[4,128,640]{1,2,0:T(8,128)(2,1)} %pad_maximum_fusion.1), calls=%async_computation.2 | async-start | bytes 1310720 | tf_op jit(solution)/shard_map/all_to_all | solution.py:41
  56.8 177.6 %all-gather.12.cloned.1.call-start = ((), (), s32[]{:S(2)}) async-start(), calls=%async_computation.7 | async-start | bytes 3932160 | tf_op jit(solution)/shard_map/all_gather | solution.py:106
  101.7 34.7 %copy-start.8 = (f32[2,4]{1,0:T(2,128)S(1)}, f32[2,4]{1,0:T(2,128)}, u32[]{:S(2)}) copy-start(f32[2,4]{1,0:T(2,128)} %param.32) | copy-start | bytes 100
  129.9 159.4 %all-gather.14.cloned.1.call-start = ((), (), s32[]{:S(2)}) async-start(), calls=%async_computation.8 | async-start | bytes 3276800 | tf_op jit(solution)/shard_map/all_gather | solution.py:99
  148.2 186.1 %reduce-scatter.2.cloned.1.call-start = ((), (), s32[]{:S(2)}) async-start(), calls=%async_computation.9 | async-start | bytes 2359296 | tf_op jit(solution)/shard_map/reduce_scatter | solution.py:192
  174.4 3.6 %collective-permute-start = (bf16[15,128]{1,0:T(8,128)(2,1)S(1)}, bf16[15,128]{1,0:T(8,128)(2,1)S(1)}, u32[]{:S(2)}, u32[]{:S(2)}) collective-permute-start(bf16[15,128]{1,0:T(8,128)(2,1)S(1)} %get-tuple-element.24), channel_id=1, source_target_pairs={{0,8},{8,16},{16,24},{1,9},{9,17},{17,25},{2,10},{10,18},{18,26},{... | collective-permute-start | bytes 11528 | tf_op jit(solution)/shard_map/ppermute | solution.py:118
  176.5 5.5 %collective-permute-start.1 = (bf16[15,128]{1,0:T(8,128)(2,1)S(1)}, bf16[15,128]{1,0:T(8,128)(2,1)S(1)}, u32[]{:S(2)}, u32[]{:S(2)}) collective-permute-start(bf16[15,128]{1,0:T(8,128)(2,1)S(1)} %get-tuple-element.25), channel_id=1, source_target_pairs={{8,0},{16,8},{24,16},{9,1},{17,9},{25,17},{10,2},{18,10},{26,18},{... | collective-permute-start | bytes 11528 | tf_op jit(solution)/shard_map/ppermute | solution.py:119
  234.5 5.4 %copy-start.9 = (bf16[2048,768]{1,0:T(8,128)(2,1)S(1)}, bf16[2048,768]{1,0:T(8,128)(2,1)}, u32[]{:S(2)}) copy-start(bf16[2048,768]{1,0:T(8,128)(2,1)} %all-gather.12.cloned.1.call-done) | copy-start | bytes 9437188
Sparse Core Ops, SparseCore 0:
  10.0 49.7 all-gather.5
  61.4 63.2 all-gather.9
  126.2 44.5 all-gather.7
  172.2 62.1 all-gather.11
  235.9 53.3 all-gather.13
  294.4 39.8 reduce-scatter.1
